TPU v7x, 32 devices: a whole 2x2x4 slice. The times are simulated.
32 devices in a mesh: grp: 2 (over y), sp: 4 (over z), tp: 4 (over x, core).
Axes of the slice: x: 2, y: 2, z: 4, core: 2. Of those that a mesh axis runs over, the one named last changes fastest.
Arguments:
- query_nope: bfloat16 [2560, 1024], P(('grp', 'sp'), 'tp'), parts along dimension 0, may hold values from -12 to 12
- query_rope: bfloat16 [2560, 512], P(('grp', 'sp'), 'tp'), parts along dimension 0, may hold values from -48 to 48
- token_latent: bfloat16 [2560, 256], P(('grp', 'sp')), parts along dimension 0, may hold values from -6 to 6
- key_rope: bfloat16 [2560, 32], P(('grp', 'sp')), parts along dimension 0, may hold values from -48 to 48
- latent_norm_gain: float32 [256], replicated, may hold values from 0.1 to 1.9
- key_expand_weight: bfloat16 [256, 1024], replicated, may hold values from -0.375 to 0.375
- value_expand_weight: bfloat16 [256, 1024], replicated, may hold values from -0.375 to 0.375
- residual: bfloat16 [2560, 2048], P(('grp', 'sp')), parts along dimension 0, may hold values from -3 to 3
- out_weight: bfloat16 [1024, 2048], P('tp'), may hold values from -0.375 to 0.375
- ffn_gain: float32 [2048], replicated, may hold values from 0.1 to 1.9
- gate_weight: bfloat16 [2048, 5632], P('sp', 'tp'), may hold values from -0.125 to 0.125
- up_weight: bfloat16 [2048, 5632], P('sp', 'tp'), may hold values from -0.125 to 0.125
- down_weight: bfloat16 [5632, 2048], P('tp', 'sp'), may hold values from -0.078125 to 0.078125
Outputs:
- layer_output: bfloat16 [2560, 2048], P(('grp', 'sp', 'tp')), parts along dimension 0
There are 2 independent parts, one for each index of `grp`. A program takes and returns all parts, laid end to end along the dimension named above; an argument that names none is the same for every part. Nothing has to cross between parts.
All inputs are finite; a program needn't handle non-finite values.
Results may differ from a plain program's by a relative error of at most 0.015.
Values may be sent and summed in bfloat16 or wider, within the bound.
A program may use at most 128 MiB of HBM per device.

v0:
```python
import jax
import jax.numpy as jnp
from jax import lax
from jax.sharding import PartitionSpec as P

UNROTATED_SIZE = 64
ROPE = 32
VALUE_SIZE = 64
GRID_W = 64


def norm_rows(values, gain):
    wide = values.astype(jnp.float32)
    return wide * lax.rsqrt(jnp.mean(wide * wide, axis=-1, keepdims=True) + 1e-06) * gain


def turn_heads(vectors, positions):
    tokens, heads, width = vectors.shape
    freqs = width // 4
    grid_pos = jnp.stack([positions // GRID_W, positions % GRID_W], axis=-1).astype(jnp.float32)
    inverse = jnp.power(10000.0, -jnp.arange(freqs, dtype=jnp.float32) / freqs)
    angles = grid_pos[:, :, None] * inverse
    cosine = jnp.cos(angles)[:, None]
    sine = jnp.sin(angles)[:, None]
    viewed = vectors.reshape(tokens, heads, 2, 2, freqs)
    first = viewed[..., 0, :]
    second = viewed[..., 1, :]
    turned = jnp.stack([first * cosine - second * sine, first * sine + second * cosine], axis=-2)
    return turned.reshape(tokens, heads, width)


def local(
    query_nope,
    query_rope,
    token_latent,
    key_rope,
    latent_norm_gain,
    key_expand_weight,
    value_expand_weight,
    residual,
    out_weight,
    ffn_gain,
    gate_weight,
    up_weight,
    down_weight,
):
    tok_rows = query_nope.shape[0]
    heads_here = query_nope.shape[1] // UNROTATED_SIZE
    own_rows = tok_rows // lax.axis_size("tp")
    tp_index = lax.axis_index("tp")
    positions = lax.axis_index("sp") * tok_rows + jnp.arange(tok_rows, dtype=jnp.int32)
    query_flat = query_nope.reshape(tok_rows, heads_here, UNROTATED_SIZE)
    query_turned = turn_heads(
        query_rope.astype(jnp.float32).reshape(tok_rows, heads_here, ROPE), positions
    ).astype(jnp.bfloat16)
    latent = norm_rows(token_latent, latent_norm_gain).astype(jnp.bfloat16)
    key_turned = turn_heads(key_rope.astype(jnp.float32)[:, None, :], positions)[:, 0].astype(
        jnp.bfloat16
    )
    key_cols = lax.dynamic_slice_in_dim(
        key_expand_weight, tp_index * heads_here * UNROTATED_SIZE, heads_here * UNROTATED_SIZE, 1
    )
    value_cols = lax.dynamic_slice_in_dim(
        value_expand_weight, tp_index * heads_here * VALUE_SIZE, heads_here * VALUE_SIZE, 1
    )
    score_scale = (UNROTATED_SIZE + ROPE) ** (-0.5)

    def absorb(carried, block_in):
        latent_block, rope_block = block_in
        block_rows = latent_block.shape[0]
        key_rows = jnp.dot(latent_block, key_cols, preferred_element_type=jnp.float32).astype(
            jnp.bfloat16
        )
        key_rows = key_rows.reshape(block_rows, heads_here, UNROTATED_SIZE)
        value_rows = jnp.dot(latent_block, value_cols, preferred_element_type=jnp.float32).astype(
            jnp.bfloat16
        )
        value_rows = value_rows.reshape(block_rows, heads_here, VALUE_SIZE)
        scores = (
            jnp.einsum("qhd,khd->hqk", query_flat, key_rows, preferred_element_type=jnp.float32)
            + jnp.einsum(
                "qhd,kd->hqk", query_turned, rope_block, preferred_element_type=jnp.float32
            )
        ) * score_scale
        highest, totals, accumulated = carried
        new_highest = jnp.maximum(highest, jnp.max(scores, axis=-1))
        shrink = jnp.exp(highest - new_highest)
        weights = jnp.exp(scores - new_highest[:, :, None])
        totals = totals * shrink + jnp.sum(weights, axis=-1)
        accumulated = accumulated * shrink.T[:, :, None] + jnp.einsum(
            "hqk,khd->qhd",
            weights.astype(jnp.bfloat16),
            value_rows,
            preferred_element_type=jnp.float32,
        )
        return ((new_highest, totals, accumulated), None)

    initial = (
        jnp.full((heads_here, tok_rows), -jnp.inf, jnp.float32),
        jnp.zeros((heads_here, tok_rows), jnp.float32),
        jnp.zeros((tok_rows, heads_here, VALUE_SIZE), jnp.float32),
    )
    carried = initial
    latent_piece = lax.all_gather(latent, "sp", axis=0, tiled=True)
    rope_piece = lax.all_gather(key_turned, "sp", axis=0, tiled=True)
    shard_count = latent_piece.shape[0] // tok_rows
    grouped = max(
        (
            factor
            for factor in range(1, shard_count + 1)
            if shard_count % factor == 0 and factor * tok_rows <= max(1024, tok_rows)
        )
    )
    block_rows = grouped * tok_rows
    blocks = (
        latent_piece.reshape(-1, block_rows, latent_piece.shape[1]),
        rope_piece.reshape(-1, block_rows, rope_piece.shape[1]),
    )
    carried, _ = lax.scan(absorb, carried, blocks)
    highest, totals, accumulated = carried
    attended = (
        (accumulated / totals.T[:, :, None])
        .reshape(tok_rows, heads_here * VALUE_SIZE)
        .astype(jnp.bfloat16)
    )
    projected = jnp.dot(attended, out_weight, preferred_element_type=jnp.float32).astype(
        jnp.bfloat16
    )
    summed = lax.psum(projected, "tp").astype(jnp.float32)
    mixed_all = residual.astype(jnp.float32) + summed
    normed_all = norm_rows(mixed_all, ffn_gain).astype(jnp.bfloat16)
    mixed_own = lax.dynamic_slice_in_dim(mixed_all, tp_index * own_rows, own_rows, 0)
    gate_piece = lax.all_gather(gate_weight, "sp", axis=0, tiled=True)
    up_piece = lax.all_gather(up_weight, "sp", axis=0, tiled=True)
    gate = jnp.dot(normed_all, gate_piece, preferred_element_type=jnp.float32)
    up_part = jnp.dot(normed_all, up_piece, preferred_element_type=jnp.float32)
    hidden = (jax.nn.silu(gate) * up_part).astype(jnp.bfloat16)
    terms = jnp.dot(
        hidden,
        lax.all_gather(down_weight, "sp", axis=1, tiled=True),
        preferred_element_type=jnp.float32,
    )
    ffn_own = lax.psum_scatter(
        terms.astype(jnp.bfloat16), "tp", scatter_dimension=0, tiled=True
    ).astype(jnp.float32)
    return (mixed_own + ffn_own).astype(jnp.bfloat16)


def solution(mesh):
    return jax.shard_map(
        local,
        mesh=mesh,
        in_specs=(
            P(("grp", "sp"), "tp"),
            P(("grp", "sp"), "tp"),
            P(("grp", "sp"), None),
            P(("grp", "sp"), None),
            P(),
            P(),
            P(),
            P(("grp", "sp"), None),
            P("tp", None),
            P(),
            P("sp", "tp"),
            P("sp", "tp"),
            P("tp", "sp"),
        ),
        out_specs=P(("grp", "sp", "tp"), None),
        check_vma=False,
    )
```

profile of v0, /device:TPU:0, one launch (start us, length us, event | category | flops | bytes accessed | tf_op | source)
XLA Modules:
  0.0 428.1 jit_solution(11533256106749414533)
XLA Ops:
  7.4 0.0 copy-start
  7.4 0.0 all-reduce.2.cloned.1.call-start
  7.4 1.1 copy.26
  8.6 0.7 convert.18
  9.3 0.2 multiply_cosine_fusion
  9.5 0.2 fusion.32
  9.7 15.1 %all-gather = bf16[4,320,32]{1,2,0:T(8,128)(2,1)S(1)} all-gather(bf16[1,320,32]{1,2,0:T(8,128)(2,1)S(1)} %bitcast.82), channel_id=1, replica_groups=mesh['grp'=2,'sp'=4,'tp'=4] {'sp'}, dimensions={0}, use_global_device_ids=true | all-gather | bytes 102400 | tf_op jit(solution)/shard_map/all_gather | solution.py:105
  24.8 0.1 copy.25
  24.8 0.1 reshape.160
  25.0 1.1 fusion.24
  26.1 1.0 fusion.26
  27.1 16.8 %all_gather.15 = bf16[1280,256]{1,0:T(8,128)(2,1)S(1)} all-gather(bf16[320,256]{1,0:T(8,128)(2,1)S(1)} %fusion.26), channel_id=1, replica_groups=mesh['grp'=2,'sp'=4,'tp'=4] {'sp'}, dimensions={0}, use_global_device_ids=true | all-gather | bytes 819200 | tf_op jit(solution)/shard_map/all_gather | solution.py:104
  43.9 0.2 copy.24
  44.2 1.0 constant_dynamic-slice_fusion
  45.2 15.2 %while.15 = (s32[]{:T(128)}, f32[4,320]{1,0:T(4,128)S(1)}, f32[4,320]{1,0:T(4,128)S(1)}, f32[320,4,64]{0,2,1:T(8,128)S(1)}, bf16[2,640,256]{2,1,0:T(8,128)(2,1)S...) while((s32[]{:T(128)}, f32[4,320]{1,0:T(4,128)S(1)}, ...), condition=%wide.region_4.5_spmd.clone, body=%wide.region_1.4_spmd.clone.sunk | while | flops 436231680 | bytes 32759976 | solution.py:119
  45.2 0.3 convolution_convert_fusion.6
  45.5 0.6 fusion.74
  46.1 2.4 fusion.75
  48.5 0.3 convolution_convert_fusion.7
  48.8 2.9 fusion.79
  51.8 1.0 fusion.77
  52.8 0.3 convolution_convert_fusion.6
  53.1 0.6 fusion.74
  53.7 2.4 fusion.75
  56.1 0.3 convolution_convert_fusion.7
  56.4 2.9 fusion.79
  59.3 1.0 fusion.77
  60.4 1.6 convolution_convert_fusion.3
  62.0 0.0 all-reduce.2.cloned.1.call-update
  62.1 0.0 all-gather.5.cloned.1.call-start
  62.1 0.5 all-gather.5.cloned.1.call-update
  62.6 0.0 all-gather.7.cloned.1.call-start
  62.7 0.5 all-gather.7.cloned.1.call-update
  63.2 0.0 all-gather.9.cloned.1.call-start
  63.3 0.5 all-gather.9.cloned.1.call-update
  63.8 0.0 copy-start.4
  63.8 0.0 reduce-scatter.2.cloned.1.call-start
  63.9 37.3 %all-reduce.2.cloned.1.call-done = bf16[320,2048]{1,0:T(8,128)(2,1)} async-done(((bf16[320,2048]{1,0:T(8,128)(2,1)}), bf16[320,2048]{1,0:T(8,128)(2,1)}) %all-reduce.2.cloned.1.call-update) | async-done | bytes 1310736 | tf_op jit(solution)/shard_map/psum | solution.py:129
  101.1 0.0 copy-done.2
  101.1 3.2 convert_add_fusion
  104.4 66.1 %all-gather.5.cloned.1.call-done = bf16[2048,1408]{1,0:T(8,128)(2,1)} async-done(((bf16[512,1408]{1,0:T(8,128)(2,1)}), bf16[2048,1408]{1,0:T(8,128)(2,1)}) %all-gather.5.cloned.1.call-update) | async-done | bytes 5767184 | tf_op jit(solution)/shard_map/all_gather | solution.py:133
  170.5 6.5 %fusion.36 = f32[320,1408]{1,0:T(8,128)} fusion(bf16[2048,1408]{1,0:T(8,128)(2,1)} %all-gather.5.cloned.1.call-done, f32[2048]{0:T(1024)S(1)} %copy-done.4, f32[320]{0:T(512)S(1)} %add_rsqrt_fusion, bf16[320,2048]{1,0:T(8,128)(2,1)} %all-reduce.2.cloned.1.call-done, bf16[320,2048]{1,0:T(8,128)(2,1)S(1)} %copy-done.2), kind=kOutput, calls=%fused_computation.69 | convolution fusion | flops 1849425920 | bytes 10200320 | tf_op jit(solution)/shard_map/dot_general | solution.py:135
  177.0 99.7 %all-gather.7.cloned.1.call-done = bf16[2048,1408]{1,0:T(8,128)(2,1)} async-done(((bf16[512,1408]{1,0:T(8,128)(2,1)}), bf16[2048,1408]{1,0:T(8,128)(2,1)}) %all-gather.7.cloned.1.call-update) | async-done | bytes 5767184 | tf_op jit(solution)/shard_map/all_gather | solution.py:134
  276.8 106.3 %all-gather.9.cloned.1.call-done = bf16[1408,2048]{1,0:T(8,128)(2,1)} async-done(((bf16[1408,512]{1,0:T(8,128)(2,1)}), bf16[1408,2048]{1,0:T(8,128)(2,1)}) %all-gather.9.cloned.1.call-update) | async-done | bytes 5767184 | tf_op jit(solution)/shard_map/all_gather | solution.py:140
  383.0 10.7 %convolution_convert_fusion.2 = bf16[320,2048]{1,0:T(8,128)(2,1)} fusion(bf16[1408,2048]{1,0:T(8,128)(2,1)} %all-gather.9.cloned.1.call-done, bf16[2048,1408]{1,0:T(8,128)(2,1)} %all-gather.7.cloned.1.call-done, f32[320,1408]{1,0:T(8,128)} %fusion.36, f32[2048]{0:T(1024)S(1)} %copy-done.4, f32[320]{0:T(512)S(1)} %add_rsqrt_fusion, ...), kind=kOutput, calls=%fused_computation.27 | convolution fusion | flops 3698278400 | bytes 17278208 | tf_op jit(solution)/shard_map/dot_general | solution.py:138
  393.7 0.0 reduce-scatter.2.cloned.1.call-update
  393.7 24.8 %reduce-scatter.2.cloned.1.call-done = bf16[80,2048]{1,0:T(8,128)(2,1)} async-done(((bf16[320,2048]{1,0:T(8,128)(2,1)}), bf16[80,2048]{1,0:T(8,128)(2,1)}) %reduce-scatter.2.cloned.1.call-update) | async-done | bytes 327696 | tf_op jit(solution)/shard_map/reduce_scatter | solution.py:143
  418.6 2.0 add_convert_fusion
  (29 shorter events, 0.3 us)
Async XLA Ops:
  7.4 53.0 %copy-start = (bf16[256,2048]{1,0:T(8,128)(2,1)S(1)}, bf16[256,2048]{1,0:T(8,128)(2,1)}, u32[]{:S(2)}) copy-start(bf16[256,2048]{1,0:T(8,128)(2,1)} %param.23) | copy-start | bytes 3145732
  7.4 36.6 %copy-start.3 = (bf16[320,256]{1,0:T(8,128)(2,1)S(1)}, bf16[320,256]{1,0:T(8,128)(2,1)}, u32[]{:S(2)}) copy-start(bf16[320,256]{1,0:T(8,128)(2,1)} %param.15) | copy-start | bytes 491524
  7.4 93.8 %all-reduce.2.cloned.1.call-start = ((), (), s32[]{:S(2)}) async-start(), calls=%async_computation.1 | async-start | bytes 2621440 | tf_op jit(solution)/shard_map/psum | solution.py:129
  48.5 3.2 copy-start.1
  56.1 3.2 copy-start.1
  62.0 39.1 %copy-start.2 = (bf16[320,2048]{1,0:T(8,128)(2,1)S(1)}, bf16[320,2048]{1,0:T(8,128)(2,1)}, u32[]{:S(2)}) copy-start(bf16[320,2048]{1,0:T(8,128)(2,1)} %param.22) | copy-start | bytes 3932164
  62.1 108.4 %all-gather.5.cloned.1.call-start = ((), (), s32[]{:S(2)}) async-start(), calls=%async_computation.2 | async-start | bytes 7208960 | tf_op jit(solution)/shard_map/all_gather | solution.py:133
  62.6 214.1 %all-gather.7.cloned.1.call-start = ((), (), s32[]{:S(2)}) async-start(), calls=%async_computation.3 | async-start | bytes 7208960 | tf_op jit(solution)/shard_map/all_gather | solution.py:134
  63.2 319.8 %all-gather.9.cloned.1.call-start = ((), (), s32[]{:S(2)}) async-start(), calls=%async_computation.4 | async-start | bytes 7208960 | tf_op jit(solution)/shard_map/all_gather | solution.py:140
  63.8 106.7 %copy-start.4 = (f32[2048]{0:T(1024)S(1)}, f32[2048]{0:T(1024)}, u32[]{:S(2)}) copy-start(f32[2048]{0:T(1024)} %param.24) | copy-start | bytes 24580
  63.8 354.8 %reduce-scatter.2.cloned.1.call-start = ((), (), s32[]{:S(2)}) async-start(), calls=%async_computation.5 | async-start | bytes 1638400 | tf_op jit(solution)/shard_map/reduce_scatter | solution.py:143
Sparse Core Ops, SparseCore 0:
  62.2 38.9 all-reduce.1
  393.8 24.6 reduce-scatter.1
Sparse Core Ops, SparseCore 1:
  64.1 106.3 all-gather.4
  171.9 104.8 all-gather.6
  278.2 104.8 all-gather.8
where the time goes:
time: 428 us
  waiting for transfers between devices  336 us (79%)
  blocking collectives  31.9 us (7%)
  matrix products  31.9 us (7%)
  between operations  15.2 us (4%)
  other arithmetic  10.5 us (2%)
    all_gather x1, waiting for transfers between devices, local(): lax.all_gather(down_weight, 'sp', axis=1, tiled=True)  106 us
    all_gather x1, waiting for transfers between devices, local(): up_piece = lax.all_gather(up_weight, 'sp', axis=0, tiled=True)  99.7 us
    all_gather x1, waiting for transfers between devices, local(): gate_piece = lax.all_gather(gate_weight, 'sp', axis=0, tiled=True)  66.1 us
    psum x1, waiting for transfers between devices, local(): summed = lax.psum(projected, 'tp').astype(jnp.float32)  37.3 us
    reduce_scatter x1, waiting for transfers between devices, local(): lax.psum_scatter(terms.astype(jnp.bfloat16), 'tp', scatter_dimension=0, t...  24.8 us
    all_gather x1, blocking collectives, local(): latent_piece = lax.all_gather(latent, 'sp', axis=0, tiled=True)  16.8 us
    all_gather x1, blocking collectives, local(): rope_piece = lax.all_gather(key_turned, 'sp', axis=0, tiled=True)  15.1 us
    dot_general x1, matrix products, local(): jnp.dot(hidden, lax.all_gather(down_weight, 'sp', axis=1, tiled=True), pr...  10.7 us
  transfers between devices with their start and end apart: 5, of which 5 were waited for; matrix products, arithmetic and copies ran while one was open for 2% of the time, Pallas kernels for 0%

commit v1 on v0

--- a/solution.py
+++ b/solution.py
@@ -126,7 +126,7 @@
     projected = jnp.dot(attended, out_weight, preferred_element_type=jnp.float32).astype(
         jnp.bfloat16
     )
-    summed = lax.psum(projected, "tp").astype(jnp.float32)
+    summed = jnp.sum(lax.all_gather(projected, "tp"), axis=0).astype(jnp.float32)
     mixed_all = residual.astype(jnp.float32) + summed
     normed_all = norm_rows(mixed_all, ffn_gain).astype(jnp.bfloat16)
     mixed_own = lax.dynamic_slice_in_dim(mixed_all, tp_index * own_rows, own_rows, 0)

time: 428 us -> 468 us (1.093)
  waiting for transfers between devices: 336 us -> 370 us
  other arithmetic: 10.5 us -> 15.9 us
    all_gather x0 -> x1, waiting for transfers between devices: none -> 38.1 us  [local(): lax.all_gather(projected, 'tp')]
    psum x1 -> x0, waiting for transfers between devices: 37.3 us -> none  [local(): summed = lax.psum(projected, 'tp').astype(jnp.float32)]
    all_gather x1, waiting for transfers between devices: 66.1 us -> 99.7 us  [local(): gate_piece = lax.all_gather(gate_weight, 'sp', axis=0, tiled=True)]
    all_gather x1, waiting for transfers between devices: 99.7 us -> 106 us  [local(): up_piece = lax.all_gather(up_weight, 'sp', axis=0, tiled=True)]
    all_gather x1, waiting for transfers between devices: 106 us -> 99.6 us  [local(): lax.all_gather(down_weight, 'sp', axis=1, tiled=True)]
    reduce_sum x0 -> x1, other arithmetic: none -> 4.96 us  [local(): jnp.sum(lax.all_gather(projected, 'tp'), axis=0).astype(jnp.float32)]
  transfers between devices with their start and end apart: 5 -> 5, of which waited for: 5 -> 5; matrix products, arithmetic and copies ran while one was open for 2% -> 3% of each run, Pallas kernels for 0% -> 0%
where the time goes in v1:
time: 468 us; the launch traced here: 467 us
  waiting for transfers between devices  370 us (79%)
  matrix products  32.6 us (7%)
  blocking collectives  31.9 us (7%)
  other arithmetic  15.9 us (3%)
  between operations  13.3 us (3%)
    all_gather x1, waiting for transfers between devices, local(): up_piece = lax.all_gather(up_weight, 'sp', axis=0, tiled=True)  106 us
    all_gather x1, waiting for transfers between devices, local(): gate_piece = lax.all_gather(gate_weight, 'sp', axis=0, tiled=True)  99.7 us
    all_gather x1, waiting for transfers between devices, local(): lax.all_gather(down_weight, 'sp', axis=1, tiled=True)  99.6 us
    all_gather x1, waiting for transfers between devices, local(): lax.all_gather(projected, 'tp')  38.1 us
    reduce_scatter x1, waiting for transfers between devices, local(): lax.psum_scatter(terms.astype(jnp.bfloat16), 'tp', scatter_dimension=0, t...  24.8 us
    all_gather x1, blocking collectives, local(): latent_piece = lax.all_gather(latent, 'sp', axis=0, tiled=True)  16.8 us
    all_gather x1, blocking collectives, local(): rope_piece = lax.all_gather(key_turned, 'sp', axis=0, tiled=True)  15.1 us
    dot_general x1, matrix products, local(): jnp.dot(hidden, lax.all_gather(down_weight, 'sp', axis=1, tiled=True), pr...  11 us
  transfers between devices with their start and end apart: 5, of which 5 were waited for; matrix products, arithmetic and copies ran while one was open for 3% of the time, Pallas kernels for 0%

profile of v1, /device:TPU:0, one launch (start us, length us, event | category | flops | bytes accessed | tf_op | source)
XLA Modules:
  0.0 467.2 jit_solution(11834628920532769985)
XLA Ops:
  6.5 0.0 copy-start
  6.6 1.1 copy.26
  7.7 0.7 convert.19
  8.5 0.2 multiply_cosine_fusion
  8.7 0.2 fusion.32
  8.9 15.1 %all-gather.1 = bf16[4,320,32]{1,2,0:T(8,128)(2,1)S(1)} all-gather(bf16[1,320,32]{1,2,0:T(8,128)(2,1)S(1)} %bitcast.84), channel_id=1, replica_groups=mesh['grp'=2,'sp'=4,'tp'=4] {'sp'}, dimensions={0}, use_global_device_ids=true | all-gather | bytes 102400 | tf_op jit(solution)/shard_map/all_gather | solution.py:105
  23.9 0.1 copy.25
  24.0 0.1 reshape.160
  24.2 1.1 fusion.24
  25.2 1.0 fusion.26
  26.3 16.8 %all_gather.21 = bf16[1280,256]{1,0:T(8,128)(2,1)S(1)} all-gather(bf16[320,256]{1,0:T(8,128)(2,1)S(1)} %fusion.26), channel_id=1, replica_groups=mesh['grp'=2,'sp'=4,'tp'=4] {'sp'}, dimensions={0}, use_global_device_ids=true | all-gather | bytes 819200 | tf_op jit(solution)/shard_map/all_gather | solution.py:104
  43.1 0.0 copy-done.2
  43.1 0.2 copy.24
  43.3 1.0 constant_dynamic-slice_fusion
  44.3 15.2 %while.15 = (s32[]{:T(128)}, f32[4,320]{1,0:T(4,128)S(1)}, f32[4,320]{1,0:T(4,128)S(1)}, f32[320,4,64]{0,2,1:T(8,128)S(1)}, bf16[2,640,256]{2,1,0:T(8,128)(2,1)S...) while((s32[]{:T(128)}, f32[4,320]{1,0:T(4,128)S(1)}, ...), condition=%wide.region_4.5_spmd.clone, body=%wide.region_1.4_spmd.clone.sunk | while | flops 436231680 | bytes 32759976 | solution.py:119
  44.3 0.3 convolution_convert_fusion.6
  44.7 0.6 fusion.74
  45.3 2.4 fusion.75
  47.7 0.3 convolution_convert_fusion.7
  48.0 2.9 fusion.79
  50.9 1.0 fusion.77
  51.9 0.3 convolution_convert_fusion.6
  52.3 0.6 fusion.74
  52.9 2.4 fusion.75
  55.3 0.3 convolution_convert_fusion.7
  55.6 2.9 fusion.79
  58.5 1.0 fusion.77
  59.6 1.6 convolution_convert_fusion.3
  61.2 0.0 all-gather.13.cloned.1.call-update
  61.2 0.0 all-gather.7.cloned.1.call-start
  61.3 0.7 all-gather.7.cloned.1.call-update
  62.0 0.0 all-gather.11.cloned.1.call-start
  62.0 0.7 all-gather.11.cloned.1.call-update
  62.7 0.0 all-gather.9.cloned.1.call-start
  62.8 0.5 all-gather.9.cloned.1.call-update
  63.3 0.2 reduce-scatter.2.cloned.1.call-start
  63.5 38.1 %all-gather.13.cloned.1.call-done = bf16[1280,2048]{1,0:T(8,128)(2,1)} async-done(((bf16[320,2048]{1,0:T(8,128)(2,1)}), bf16[1280,2048]{1,0:T(8,128)(2,1)}) %all-gather.13.cloned.1.call-update) | async-done | bytes 5242896 | tf_op jit(solution)/shard_map/all_gather | solution.py:129
  101.6 5.0 %reduce_sum.40 = bf16[320,2048]{1,0:T(8,128)(2,1)} reduce(bf16[4,320,2048]{2,1,0:T(8,128)(2,1)} %bitcast.79, bf16[]{:T(256)} %constant.85.clone.1), dimensions={0}, to_apply=%region_5.6 | reduce | flops 1966080 | bytes 6553602 | tf_op jit(solution)/shard_map/reduce_sum | solution.py:129
  106.6 3.6 convert_add_fusion
  110.2 99.7 %all-gather.7.cloned.1.call-done = bf16[2048,1408]{1,0:T(8,128)(2,1)} async-done(((bf16[512,1408]{1,0:T(8,128)(2,1)}), bf16[2048,1408]{1,0:T(8,128)(2,1)}) %all-gather.7.cloned.1.call-update) | async-done | bytes 5767184 | tf_op jit(solution)/shard_map/all_gather | solution.py:133
  209.9 0.0 copy-done.3
  209.9 6.9 %fusion.36 = f32[320,1408]{1,0:T(8,128)} fusion(bf16[2048,1408]{1,0:T(8,128)(2,1)} %all-gather.7.cloned.1.call-done, f32[2048]{0:T(1024)S(1)} %copy-done.3, f32[320]{0:T(512)S(1)} %add_rsqrt_fusion, bf16[320,2048]{1,0:T(8,128)(2,1)} %reduce_sum.40, bf16[320,2048]{1,0:T(8,128)(2,1)} %param.22), kind=kOutput, calls=%fused_computation.69 | convolution fusion | flops 1849425920 | bytes 10200320 | tf_op jit(solution)/shard_map/dot_general | solution.py:135
  216.8 99.6 %all-gather.11.cloned.1.call-done = bf16[1408,2048]{1,0:T(8,128)(2,1)} async-done(((bf16[1408,512]{1,0:T(8,128)(2,1)}), bf16[1408,2048]{1,0:T(8,128)(2,1)}) %all-gather.11.cloned.1.call-update) | async-done | bytes 5767184 | tf_op jit(solution)/shard_map/all_gather | solution.py:140
  316.4 106.4 %all-gather.9.cloned.1.call-done = bf16[2048,1408]{1,0:T(8,128)(2,1)} async-done(((bf16[512,1408]{1,0:T(8,128)(2,1)}), bf16[2048,1408]{1,0:T(8,128)(2,1)}) %all-gather.9.cloned.1.call-update) | async-done | bytes 5767184 | tf_op jit(solution)/shard_map/all_gather | solution.py:134
  422.8 11.0 %convolution_convert_fusion.2 = bf16[320,2048]{1,0:T(8,128)(2,1)} fusion(bf16[1408,2048]{1,0:T(8,128)(2,1)} %all-gather.11.cloned.1.call-done, bf16[2048,1408]{1,0:T(8,128)(2,1)} %all-gather.9.cloned.1.call-done, f32[320,1408]{1,0:T(8,128)} %fusion.36, f32[2048]{0:T(1024)S(1)} %copy-done.3, f32[320]{0:T(512)S(1)} %add_rsqrt_fusion, ...), kind=kOutput, calls=%fused_computation.27 | convolution fusion | flops 3698278400 | bytes 17278208 | tf_op jit(solution)/shard_map/dot_general | solution.py:138
  433.9 0.0 reduce-scatter.2.cloned.1.call-update
  433.9 24.8 %reduce-scatter.2.cloned.1.call-done = bf16[80,2048]{1,0:T(8,128)(2,1)} async-done(((bf16[320,2048]{1,0:T(8,128)(2,1)}), bf16[80,2048]{1,0:T(8,128)(2,1)}) %reduce-scatter.2.cloned.1.call-update) | async-done | bytes 327696 | tf_op jit(solution)/shard_map/reduce_scatter | solution.py:143
  458.7 2.0 add_convert_fusion
  (28 shorter events, 0.3 us)
Async XLA Ops:
  6.5 53.0 %copy-start = (bf16[256,2048]{1,0:T(8,128)(2,1)S(1)}, bf16[256,2048]{1,0:T(8,128)(2,1)}, u32[]{:S(2)}) copy-start(bf16[256,2048]{1,0:T(8,128)(2,1)} %param.23) | copy-start | bytes 3145732
  6.5 36.6 %copy-start.2 = (bf16[320,256]{1,0:T(8,128)(2,1)S(1)}, bf16[320,256]{1,0:T(8,128)(2,1)}, u32[]{:S(2)}) copy-start(bf16[320,256]{1,0:T(8,128)(2,1)} %param.15) | copy-start | bytes 491524
  6.5 95.0 %all-gather.13.cloned.1.call-start = ((), (), s32[]{:S(2)}) async-start(), calls=%async_computation.5 | async-start | bytes 6553600 | tf_op jit(solution)/shard_map/all_gather | solution.py:129
  47.7 3.3 copy-start.1
  55.3 3.3 copy-start.1
  61.2 148.7 %all-gather.7.cloned.1.call-start = ((), (), s32[]{:S(2)}) async-start(), calls=%async_computation.1 | async-start | bytes 7208960 | tf_op jit(solution)/shard_map/all_gather | solution.py:133
  62.0 254.5 %all-gather.11.cloned.1.call-start = ((), (), s32[]{:S(2)}) async-start(), calls=%async_computation.3 | async-start | bytes 7208960 | tf_op jit(solution)/shard_map/all_gather | solution.py:140
  62.7 360.1 %all-gather.9.cloned.1.call-start = ((), (), s32[]{:S(2)}) async-start(), calls=%async_computation.2 | async-start | bytes 7208960 | tf_op jit(solution)/shard_map/all_gather | solution.py:134
  63.3 395.4 %reduce-scatter.2.cloned.1.call-start = ((), (), s32[]{:S(2)}) async-start(), calls=%async_computation.4 | async-start | bytes 1638400 | tf_op jit(solution)/shard_map/reduce_scatter | solution.py:143
  106.5 103.3 %copy-start.3 = (f32[2048]{0:T(1024)S(1)}, f32[2048]{0:T(1024)}, u32[]{:S(2)}) copy-start(f32[2048]{0:T(1024)} %param.24) | copy-start | bytes 24580
Sparse Core Ops, SparseCore 0:
  61.3 40.1 all-gather.12
  103.2 106.6 all-gather.6
  211.5 104.9 all-gather.10
  317.9 104.9 all-gather.8
  434.0 24.6 reduce-scatter.1
